TPU v7x, 32 devices: a whole 2x2x4 slice. The times are simulated.
32 devices in a mesh: sp: 16 (over z, y, x), tp: 2 (over core).
Axes of the slice: x: 2, y: 2, z: 4, core: 2. Of those that a mesh axis runs over, the one named last changes fastest.
Arguments:
- glu_value: bfloat16 [4096, 1024], P('sp', 'tp'), may hold values from -12 to 12
- glu_gate: bfloat16 [4096, 1024], P('sp', 'tp'), may hold values from -8 to 8
- conv_kernel: bfloat16 [31, 1024], P(None, 'tp'), may hold values from -1 to 1
- conv_bias: float32 [1024], P('tp'), may hold values from -1.5 to 1.5
- group_gain: float32 [1024], P('tp'), may hold values from 0.1 to 1.9
- group_shift: float32 [1024], P('tp'), may hold values from -2.5 to 2.5
- out_weight: bfloat16 [1024, 2048], replicated, may hold values from -0.1875 to 0.1875
- residual: bfloat16 [4096, 2048], P(('sp', 'tp')), may hold values from -12 to 12
- ffn_gain: float32 [2048], replicated, may hold values from 0.1 to 1.9
- expert_pick: int32 [4096, 2], P(('sp', 'tp')), may hold values from 0 to 31, as said below
- pair_logits: float32 [4096, 2], P(('sp', 'tp')), may hold values from -1.2 to 1.2
- group_prob: float32 [4096], P(('sp', 'tp')), may hold values from 0.5 to 1
- gate_weight: bfloat16 [32, 2048, 512], P(('sp', 'tp')), may hold values from -0.125 to 0.125
- up_weight: bfloat16 [32, 2048, 512], P(('sp', 'tp')), may hold values from -0.125 to 0.125
- down_weight: bfloat16 [32, 512, 2048], P(('sp', 'tp')), may hold values from -0.75 to 0.75
Outputs:
- result: bfloat16 [4096, 2048], P(('sp', 'tp'))
Inputs may be any that keep to these rules, and one draw needn't show every extreme that they name: `expert_pick`: both picks of a token are different experts of the same group of 8 consecutive experts. Among the 128 tokens of one device (aligned blocks of rows) no expert is picked more than 16 times, and in every such block some expert is picked exactly 16 times.
All inputs are finite; a program needn't handle non-finite values.
Results may differ from a plain program's by a relative error of at most 0.014.
Values may be sent and summed in bfloat16 or wider, within the bound.
A program may use at most 64 MiB of HBM per device.

v0:
```python
import functools

import jax
import jax.numpy as jnp
from jax import lax
from jax.experimental import pallas as pl
from jax.experimental.pallas import tpu as pltpu
from jax.sharding import PartitionSpec as P

CONV_GROUPS = 8


EPS = 1e-06


PLANES = 4
MESH = pl.DeviceIdType.MESH
ORDER = (1, 3, 2)
ROWS_MIN = 16
HALVES = 2


def layer_kernel(
    cap,
    slot,
    value_ref,
    gate_ref,
    taps_ref,
    bias_ref,
    gain_ref,
    shift_ref,
    residual_ref,
    ffn_ref,
    pick_ref,
    logit_ref,
    prob_ref,
    out_hbm,
    gate_hbm,
    up_hbm,
    down_hbm,
    out_ref,
    glued,
    hsend,
    hrecv,
    mixed,
    mrest,
    place_ref,
    meta_ref,
    normed_ref,
    hidden_ref,
    proj,
    out_v,
    zsend,
    zrecv,
    mrecv,
    xsend,
    xrecv,
    asend,
    arecv,
    csend,
    cret,
    gate_v,
    up_v,
    down_v,
    wsem,
    hss,
    hrs,
    tss,
    trs,
    zss,
    zrs,
    mss,
    mrs,
    xss,
    xrs,
    ass,
    ars,
    css,
    crs,
):
    n_tp = lax.axis_size("tp")
    chips = lax.axis_size("sp") // PLANES
    peers = chips * n_tp
    sp = lax.axis_index("sp")
    tp = lax.axis_index("tp")
    n_sp = lax.axis_size("sp")
    z = sp // chips
    here = sp % chips
    tokens = residual_ref.shape[0]
    length, channels = value_ref.shape
    reach = taps_ref.shape[0] - 1
    lead = hsend.shape[0]
    j = here * n_tp + tp
    slots = peers * slot
    group_rows = zsend.shape[2]
    half = zsend.shape[3]

    def span(h):
        return slice(h * half, (h + 1) * half)

    def plane(d):
        if d == 1:
            return z + 1 - 2 * (z % 2)
        if d == 2:
            return z + 2 - 4 * (z // 2)
        return PLANES - 1 - z

    def mate(d):
        return (plane(d) * chips + here, tp)

    def peer(k):
        return (z * chips + k // n_tp, k % n_tp)

    def zcopy(d, h):
        return pltpu.make_async_remote_copy(
            src_ref=zsend.at[d, h], dst_ref=zrecv.at[d, h],
            send_sem=zss.at[d, h], recv_sem=zrs.at[d, h],
            device_id=mate(d), device_id_type=MESH,
        )

    def mcopy(d):
        return pltpu.make_async_remote_copy(
            src_ref=meta_ref.at[d], dst_ref=mrecv.at[d], send_sem=mss.at[d], recv_sem=mrs.at[d],
            device_id=mate(d), device_id_type=MESH,
        )

    def ccopy(d, h):
        return pltpu.make_async_remote_copy(
            src_ref=csend.at[d, h], dst_ref=cret.at[d, h],
            send_sem=css.at[d, h], recv_sem=crs.at[d, h],
            device_id=mate(d), device_id_type=MESH,
        )

    def xcopy(d, h, o):
        rows = pl.ds(o * slot, slot)
        return pltpu.make_async_remote_copy(
            src_ref=xsend.at[d, h, rows], dst_ref=xrecv.at[d, h, rows],
            send_sem=xss.at[d, h, o], recv_sem=xrs.at[d, h, o],
            device_id=peer((j + o) % peers), device_id_type=MESH,
        )

    def acopy(d, h, o):
        rows = pl.ds(o * slot, slot)
        return pltpu.make_async_remote_copy(
            src_ref=asend.at[d, h, rows], dst_ref=arecv.at[d, h, rows],
            send_sem=ass.at[d, h, o], recv_sem=ars.at[d, h, o],
            device_id=peer((j + peers - o) % peers), device_id_type=MESH,
        )

    def halo():
        return pltpu.make_async_remote_copy(
            src_ref=hsend, dst_ref=hrecv, send_sem=hss.at[0], recv_sem=hrs.at[0],
            device_id=((sp + 1) % n_sp, tp), device_id_type=MESH,
        )

    def tcopy(o):
        other = (tp + o) % n_tp
        rows = pl.ds(pl.multiple_of(other * tokens, tokens), tokens)
        return pltpu.make_async_remote_copy(
            src_ref=mixed.at[rows], dst_ref=mrest.at[o], send_sem=tss.at[o], recv_sem=trs.at[o],
            device_id=(sp, other), device_id_type=MESH,
        )

    out_copy = pltpu.make_async_copy(out_hbm, out_v, wsem.at[3])
    out_copy.start()
    weights = [
        pltpu.make_async_copy(gate_hbm.at[0], gate_v, wsem.at[0]),
        pltpu.make_async_copy(up_hbm.at[0], up_v, wsem.at[1]),
        pltpu.make_async_copy(down_hbm.at[0], down_v, wsem.at[2]),
    ]
    for copy in weights:
        copy.start()

    barrier = pltpu.get_barrier_semaphore()
    for d in ORDER:
        pl.semaphore_signal(barrier, inc=1, device_id=mate(d), device_id_type=MESH)
    for o in range(1, peers):
        pl.semaphore_signal(
            barrier, inc=1, device_id=peer((j + o) % peers), device_id_type=MESH
        )
    pl.semaphore_signal(
        barrier, inc=1, device_id=((sp + 1) % n_sp, tp), device_id_type=MESH
    )
    pl.semaphore_signal(
        barrier, inc=1, device_id=((sp + n_sp - 1) % n_sp, tp), device_id_type=MESH
    )

    f32 = jnp.float32
    bf16 = jnp.bfloat16
    block = 64
    for start in range(length - block, -1, -block):
        rows = slice(start, start + block)
        gated = value_ref[rows].astype(f32) / (1.0 + jnp.exp(-gate_ref[rows].astype(f32)))
        gated = gated.astype(bf16)
        glued[lead + start : lead + start + block] = gated.astype(f32)
        if start == length - block:
            hsend[...] = gated[block - lead :]
    pl.semaphore_wait(barrier, len(ORDER) + peers + 1)
    halo().start()

    lane = lax.broadcasted_iota(jnp.int32, (tokens, 128), 1)
    picks = pick_ref[...].astype(f32)
    logits = logit_ref[...]
    cols = [picks[:, 0:1], picks[:, 1:2], logits[:, 0:1], logits[:, 1:2]]
    wide = jnp.zeros((tokens, 128), f32)
    for k in range(4):
        wide = jnp.where(lane == k, cols[k], wide)
    tall = wide.T
    rows_of = [tall[k : k + 1, :] for k in range(4)]
    square = (tokens, tokens)
    earlier = lax.broadcasted_iota(jnp.int32, square, 0) < lax.broadcasted_iota(
        jnp.int32, square, 1
    )

    def group_of(pick):
        total = jnp.zeros(pick.shape, f32)
        for q in range(1, PLANES):
            total += jnp.where(pick >= (q * peers), 1.0, 0.0)
        return total

    def count(hit):
        return jnp.sum(jnp.where(hit & earlier, 1.0, 0.0), axis=0, keepdims=True)

    ranks = [count((cols[0] == r) | (cols[1] == r)) for r in rows_of[:2]]
    group_row = group_of(rows_of[0])
    spot = count(group_of(cols[0]) == group_row)
    away = group_row.astype(jnp.int32) ^ z
    at_row = away.astype(f32) * group_rows + spot
    row_id = lax.broadcasted_iota(jnp.int32, (PLANES * group_rows, tokens), 0).astype(f32)
    place_ref[...] = jnp.where(row_id == at_row, 1.0, 0.0).astype(bf16)
    gap = rows_of[2] - rows_of[3]
    shares = [prob_ref[...] / (1.0 + jnp.exp(-gap)), prob_ref[...] / (1.0 + jnp.exp(gap))]
    fields = [jnp.ones((1, tokens), f32)]
    for k in range(2):
        fields += [rows_of[k] - group_row * peers, ranks[k]]
    for share in shares:
        for _ in range(3):
            part = share.astype(bf16).astype(f32)
            fields.append(part)
            share = share - part
    field_id = lax.broadcasted_iota(jnp.int32, (16, tokens), 0)
    table = jnp.zeros((16, tokens), f32)
    for k, field in enumerate(fields):
        table = jnp.where(field_id == k, field, table)
    table = table.astype(bf16)
    meta_ref[...] = jnp.zeros(meta_ref.shape, f32)
    for d in range(PLANES):
        part = lax.dot_general(
            table,
            place_ref[d * group_rows : (d + 1) * group_rows, :],
            (((1,), (1,)), ((), ())),
            preferred_element_type=f32,
        )
        empty = (1.0 - part[0:1]) * 65536.0
        meta_ref[d, 0:1, :group_rows] = part[1:2] * slot + part[2:3] + empty
        meta_ref[d, 1:2, :group_rows] = part[3:4] * slot + part[4:5] + empty
        meta_ref[d, 2:3, :group_rows] = part[5:6] + part[6:7] + part[7:8]
        meta_ref[d, 3:4, :group_rows] = part[8:9] + part[9:10] + part[10:11]
    for d in ORDER:
        mcopy(d).start()

    wide_group = channels * n_tp // CONV_GROUPS
    taps = taps_ref[...].astype(f32)
    for start in range(length - block, -1, -block):
        if start == 0:
            halo().wait_recv()
            keep = jnp.where(sp > 0, 1.0, 0.0)
            glued[:lead] = hrecv[...].astype(f32) * keep
        for low_lane in range(0, channels, wide_group):
            part = slice(low_lane, low_lane + wide_group)
            total = jnp.zeros((block, wide_group), f32) + bias_ref[:, part]
            for offset in range(reach + 1):
                first = start + lead - reach + offset
                total += taps[offset : offset + 1, part] * glued[first : first + block, part]
            centre = jnp.mean(total, axis=-1, keepdims=True)
            total = total - centre
            variance = jnp.mean(total * total, axis=-1, keepdims=True)
            level = total * lax.rsqrt(variance + EPS)
            level = level * gain_ref[:, part] + shift_ref[:, part]
            mixed[start : start + block, part] = (level / (1.0 + jnp.exp(-level))).astype(bf16)
    for o in range(1, n_tp):
        tcopy(o).start()
    out_copy.wait()

    def weight_rows(which):
        return out_v[pl.ds(pl.multiple_of(which * channels, channels), channels), :]

    own = mixed[pl.ds(pl.multiple_of(tp * tokens, tokens), tokens), :]
    proj[...] = jnp.dot(own, weight_rows(tp), preferred_element_type=f32)
    for o in range(1, n_tp):
        tcopy(o).wait_recv()
        proj[...] += jnp.dot(
            mrest[o], weight_rows((tp + n_tp - o) % n_tp), preferred_element_type=f32
        )
    for start in range(0, tokens, 16):
        rows = slice(start, start + 16)
        hidden = (residual_ref[rows].astype(f32) + proj[rows]).astype(bf16)
        hidden_ref[rows] = hidden
        full = hidden.astype(f32)
        scale = lax.rsqrt(jnp.mean(full * full, axis=-1, keepdims=True) + EPS)
        normed_ref[rows] = (full * scale * ffn_ref[...]).astype(bf16)

    for d in ORDER + (0,):
        for h in range(HALVES):
            picked = jnp.dot(
                place_ref[d * group_rows : (d + 1) * group_rows, :],
                normed_ref[:, span(h)],
                preferred_element_type=f32,
            )
            zsend[d, h] = picked.astype(bf16)
            if d:
                zcopy(d, h).start()

    def places(d):
        meta = meta_ref[0] if d == 0 else mrecv[d]
        row = lax.broadcasted_iota(jnp.int32, (slots, group_rows), 0).astype(jnp.float32)
        shift = (j * slot).astype(jnp.float32)
        out = []
        for k in range(2):
            at = meta[k : k + 1, :group_rows] - shift
            at = jnp.where(at < 0, at + slots, at)
            out.append(row == at)
        shares = [meta[2 + k : 3 + k, :group_rows] for k in range(2)]
        return out, shares

    def entry(d):
        if d:
            mcopy(d).wait_recv()
        at, _ = places(d)
        chosen = jnp.where(at[0] | at[1], 1.0, 0.0).astype(jnp.bfloat16)
        for h in range(HALVES):
            if d:
                zcopy(d, h).wait_recv()
            rows = zsend[0, h] if d == 0 else zrecv[d, h]
            spread = jnp.dot(chosen, rows, preferred_element_type=jnp.float32)
            spread = spread.astype(jnp.bfloat16)
            xrecv[d, h, :slot] = spread[:slot]
            xsend[d, h, slot:] = spread[slot:]
            for o in range(1, peers):
                xcopy(d, h, o).start()

    def expert(d):
        gate_out = None
        for h in range(HALVES):
            for o in range(1, peers):
                xcopy(d, h, o).wait_recv()
            rows = xrecv[d, h]
            gate_part = jnp.dot(rows, gate_v[span(h), :], preferred_element_type=jnp.float32)
            up_part = jnp.dot(rows, up_v[span(h), :], preferred_element_type=jnp.float32)
            gate_out = gate_part if h == 0 else gate_out + gate_part
            up_out = up_part if h == 0 else up_out + up_part
        active = (gate_out / (1.0 + jnp.exp(-gate_out)) * up_out).astype(jnp.bfloat16)
        for h in range(HALVES):
            answer = jnp.dot(active, down_v[:, span(h)], preferred_element_type=jnp.float32)
            answer = answer.astype(jnp.bfloat16)
            arecv[d, h, :slot] = answer[:slot]
            asend[d, h, slot:] = answer[slot:]
            for o in range(1, peers):
                acopy(d, h, o).start()

    def combine(d):
        at, shares = places(d)
        mix = jnp.where(at[0], shares[0], 0.0) + jnp.where(at[1], shares[1], 0.0)
        high = mix.astype(jnp.bfloat16)
        low = (mix - high.astype(jnp.float32)).astype(jnp.bfloat16)
        dims = (((0,), (0,)), ((), ()))
        for h in range(HALVES):
            for o in range(1, peers):
                acopy(d, h, o).wait_recv()
            answers = arecv[d, h]
            total = lax.dot_general(high, answers, dims, preferred_element_type=jnp.float32)
            total += lax.dot_general(low, answers, dims, preferred_element_type=jnp.float32)
            if d == 0:
                cret[0, h] = total.astype(jnp.bfloat16)
            else:
                csend[d, h] = total.astype(jnp.bfloat16)
                ccopy(d, h).start()

    a, b, c = ORDER
    entry(0)
    entry(a)
    for copy in weights:
        copy.wait()
    expert(0)
    entry(b)
    inner = (z >= 1) & (z < PLANES - 1)

    @pl.when(inner)
    def _():
        expert(a)
        combine(0)
        expert(b)
        combine(a)
        combine(b)
        entry(c)
        expert(c)
        combine(c)

    @pl.when(jnp.logical_not(inner))
    def _():
        expert(a)
        combine(0)
        entry(c)
        combine(a)
        expert(b)
        expert(c)
        combine(b)
        combine(c)

    dims = (((0,), (0,)), ((), ()))
    for h in range(HALVES):
        total = hidden_ref[:, span(h)].astype(jnp.float32)
        for d in (0,) + ORDER:
            if d:
                ccopy(d, h).wait_recv()
            total += lax.dot_general(
                place_ref[d * group_rows : (d + 1) * group_rows, :],
                cret[d, h],
                dims,
                preferred_element_type=jnp.float32,
            )
        out_ref[:, span(h)] = total.astype(jnp.bfloat16)

    halo().wait_send()
    for o in range(1, n_tp):
        tcopy(o).wait_send()
    for d in ORDER:
        mcopy(d).wait_send()
        for h in range(HALVES):
            zcopy(d, h).wait_send()
            ccopy(d, h).wait_send()
    for d in range(PLANES):
        for h in range(HALVES):
            for o in range(1, peers):
                xcopy(d, h, o).wait_send()
                acopy(d, h, o).wait_send()


def local(
    glu_value,
    glu_gate,
    conv_kernel,
    conv_bias,
    group_gain,
    group_shift,
    out_weight,
    residual,
    ffn_gain,
    expert_pick,
    pair_logits,
    group_prob,
    gate_weight,
    up_weight,
    down_weight,
):
    rows, width = residual.shape
    length, channels = glu_value.shape
    n_tp = lax.axis_size("tp")
    experts_all = lax.axis_size("sp") * n_tp
    cap = 4 * rows // experts_all
    peers = experts_all // PLANES
    group_rows = peers * cap // 2
    slot = max(cap, ROWS_MIN)
    slots = peers * slot
    lead = -(-(conv_kernel.shape[0] - 1) // 16) * 16
    bf16 = jnp.bfloat16
    f32 = jnp.float32
    vmem = pl.BlockSpec(memory_space=pltpu.VMEM)
    hbm = pl.BlockSpec(memory_space=pl.ANY)
    dma = pltpu.SemaphoreType.DMA
    return pl.pallas_call(
        functools.partial(layer_kernel, cap, slot),
        out_shape=jax.ShapeDtypeStruct((rows, width), bf16),
        in_specs=[vmem] * 11 + [hbm] * 4,
        out_specs=vmem,
        scratch_shapes=[
            pltpu.VMEM((lead + length, channels), f32),
            pltpu.VMEM((lead, channels), bf16),
            pltpu.VMEM((lead, channels), bf16),
            pltpu.VMEM((length, channels), bf16),
            pltpu.VMEM((n_tp, rows, channels), bf16),
            pltpu.VMEM((PLANES * group_rows, rows), bf16),
            pltpu.VMEM((PLANES, 8, 128), f32),
            pltpu.VMEM((rows, width), bf16),
            pltpu.VMEM((rows, width), bf16),
            pltpu.VMEM((rows, width), f32),
            pltpu.VMEM(out_weight.shape, bf16),
            pltpu.VMEM((PLANES, HALVES, group_rows, width // HALVES), bf16),
            pltpu.VMEM((PLANES, HALVES, group_rows, width // HALVES), bf16),
            pltpu.VMEM((PLANES, 8, 128), f32),
            pltpu.VMEM((PLANES, HALVES, slots, width // HALVES), bf16),
            pltpu.VMEM((PLANES, HALVES, slots, width // HALVES), bf16),
            pltpu.VMEM((PLANES, HALVES, slots, width // HALVES), bf16),
            pltpu.VMEM((PLANES, HALVES, slots, width // HALVES), bf16),
            pltpu.VMEM((PLANES, HALVES, group_rows, width // HALVES), bf16),
            pltpu.VMEM((PLANES, HALVES, group_rows, width // HALVES), bf16),
            pltpu.VMEM(gate_weight.shape[1:], bf16),
            pltpu.VMEM(up_weight.shape[1:], bf16),
            pltpu.VMEM(down_weight.shape[1:], bf16),
            dma((4,)),
            dma((1,)),
            dma((1,)),
            dma((n_tp,)),
            dma((n_tp,)),
            dma((PLANES, HALVES)),
            dma((PLANES, HALVES)),
            dma((PLANES,)),
            dma((PLANES,)),
            dma((PLANES, HALVES, peers)),
            dma((PLANES, HALVES, peers)),
            dma((PLANES, HALVES, peers)),
            dma((PLANES, HALVES, peers)),
            dma((PLANES, HALVES)),
            dma((PLANES, HALVES)),
        ],
        compiler_params=pltpu.CompilerParams(
            collective_id=0, has_side_effects=True, vmem_limit_bytes=62 * 1024 * 1024
        ),
    )(
        glu_value,
        glu_gate,
        conv_kernel,
        conv_bias[None, :],
        group_gain[None, :],
        group_shift[None, :],
        residual,
        ffn_gain[None, :],
        expert_pick,
        pair_logits,
        group_prob[None, :],
        out_weight,
        gate_weight,
        up_weight,
        down_weight,
    )


def solution(mesh):
    in_specs = (
        P("sp", "tp"),
        P("sp", "tp"),
        P(None, "tp"),
        P("tp"),
        P("tp"),
        P("tp"),
        P(),
        P(("sp", "tp"), None),
        P(),
        P(("sp", "tp"), None),
        P(("sp", "tp"), None),
        P(("sp", "tp")),
        P(("sp", "tp"), None, None),
        P(("sp", "tp"), None, None),
        P(("sp", "tp"), None, None),
    )
    out_specs = P(("sp", "tp"), None)
    return jax.shard_map(local, mesh=mesh, in_specs=in_specs, out_specs=out_specs, check_vma=False)
```

profile of v0, /device:TPU:0, one launch (start us, length us, event | category | flops | bytes accessed | tf_op | source)
XLA Modules:
  0.0 80.7 jit_solution(15045234610261575073)
XLA Ops:
  0.0 1.4 %copy.16.pick_ref = s32[128,2]{1,0:T(8,128)} copy(s32[128,2]{0,1:T(2,128)} %param.24) | data formatting | bytes 2048 | tf_op args[9]
  1.4 1.4 %copy.17.logit_ref = f32[128,2]{1,0:T(8,128)} copy(f32[128,2]{0,1:T(2,128)} %param.25) | data formatting | bytes 2048 | tf_op args[10]
  2.8 76.0 %shard_map.145 = bf16[128,2048]{1,0:T(8,128)(2,1)} custom-call(bf16[256,512]{1,0:T(8,128)(2,1)} %value_ref.1, bf16[256,512]{1,0:T(8,128)(2,1)} %gate_ref.1, bf16[31,512]{1,0:T(8,128)(2,1)} %taps_ref.1, f32[1,512]{1,0:T(1,128)} %bitcast.6, f32[1,512]{1,0:T(1,128)} %bitcast.7, f32[1,512]{1,0:T(1,128)} %bitcast.8, bf16[128,2048]{1,0:T(8,128)(2,1)} %residual_ref.1, ...), custom_call_target="tpu_custom_call" | custom-call | tf_op jit(solution)/shard_map/pallas_call | solution.py:471
  78.8 1.9 %copy.19 = bf16[128,2048]{1,0:T(8,128)(2,1)} copy(bf16[128,2048]{1,0:T(8,128)(2,1)} %shard_map.145) | data formatting | bytes 1048576
where the time goes:
time: 80.9 us; the launch traced here: 80.7 us
  Pallas kernels  76 us (94%)
  local copies, waits for them, and re-layouts  4.7 us (6%)
    pallas_call x1, Pallas kernels, local(): pl.pallas_call(functools.partial(layer_kernel, cap, slot), out_shape=jax....  76 us
    unnamed x3, local copies, waits for them, and re-layouts  4.7 us

commit v1 on v0

--- a/solution.py
+++ b/solution.py
@@ -23,6 +23,22 @@
 def layer_kernel(
     cap,
     slot,
+    value_hbm,
+    glu_gate_hbm,
+    taps_hbm,
+    bias_hbm,
+    gain_hbm,
+    shift_hbm,
+    residual_hbm,
+    ffn_hbm,
+    pick_hbm,
+    logit_hbm,
+    prob_hbm,
+    out_hbm,
+    gate_hbm,
+    up_hbm,
+    down_hbm,
+    out_ref,
     value_ref,
     gate_ref,
     taps_ref,
@@ -34,11 +50,7 @@
     pick_ref,
     logit_ref,
     prob_ref,
-    out_hbm,
-    gate_hbm,
-    up_hbm,
-    down_hbm,
-    out_ref,
+    isem,
     glued,
     hsend,
     hrecv,
@@ -153,24 +165,19 @@
             device_id=((sp + 1) % n_sp, tp), device_id_type=MESH,
         )
 
-    def tcopy(o):
+    block = 64
+
+    def tcopy(o, begin, size):
         other = (tp + o) % n_tp
-        rows = pl.ds(pl.multiple_of(other * tokens, tokens), tokens)
+        rows = pl.ds(pl.multiple_of(other * tokens + begin, size), size)
+        mark = begin // (block // 2)
         return pltpu.make_async_remote_copy(
-            src_ref=mixed.at[rows], dst_ref=mrest.at[o], send_sem=tss.at[o], recv_sem=trs.at[o],
+            src_ref=mixed.at[rows], dst_ref=mrest.at[o, pl.ds(begin, size)],
+            send_sem=tss.at[o, mark], recv_sem=trs.at[o, mark],
             device_id=(sp, other), device_id_type=MESH,
         )
 
-    out_copy = pltpu.make_async_copy(out_hbm, out_v, wsem.at[3])
-    out_copy.start()
-    weights = [
-        pltpu.make_async_copy(gate_hbm.at[0], gate_v, wsem.at[0]),
-        pltpu.make_async_copy(up_hbm.at[0], up_v, wsem.at[1]),
-        pltpu.make_async_copy(down_hbm.at[0], down_v, wsem.at[2]),
-    ]
-    for copy in weights:
-        copy.start()
-
+    head_dev, tail_dev = sp == 0, sp == n_sp - 1
     barrier = pltpu.get_barrier_semaphore()
     for d in ORDER:
         pl.semaphore_signal(barrier, inc=1, device_id=mate(d), device_id_type=MESH)
@@ -178,16 +185,35 @@
         pl.semaphore_signal(
             barrier, inc=1, device_id=peer((j + o) % peers), device_id_type=MESH
         )
-    pl.semaphore_signal(
-        barrier, inc=1, device_id=((sp + 1) % n_sp, tp), device_id_type=MESH
+
+    @pl.when(jnp.logical_not(tail_dev))
+    def _():
+        pl.semaphore_signal(barrier, inc=1, device_id=(sp + 1, tp), device_id_type=MESH)
+
+    @pl.when(jnp.logical_not(head_dev))
+    def _():
+        pl.semaphore_signal(barrier, inc=1, device_id=(sp - 1, tp), device_id_type=MESH)
+
+    sources = (
+        (value_hbm, value_ref), (glu_gate_hbm, gate_ref), (pick_hbm, pick_ref),
+        (logit_hbm, logit_ref), (prob_hbm, prob_ref), (taps_hbm, taps_ref),
+        (bias_hbm, bias_ref), (gain_hbm, gain_ref), (shift_hbm, shift_ref),
+        (ffn_hbm, ffn_ref), (residual_hbm, residual_ref),
     )
-    pl.semaphore_signal(
-        barrier, inc=1, device_id=((sp + n_sp - 1) % n_sp, tp), device_id_type=MESH
-    )
-
+    inputs = [pltpu.make_async_copy(a, b, isem.at[k]) for k, (a, b) in enumerate(sources)]
+    for copy in inputs:
+        copy.start()
+    out_copy = pltpu.make_async_copy(out_hbm, out_v, wsem.at[3])
+    weights = [
+        pltpu.make_async_copy(gate_hbm.at[0], gate_v, wsem.at[0]),
+        pltpu.make_async_copy(up_hbm.at[0], up_v, wsem.at[1]),
+        pltpu.make_async_copy(down_hbm.at[0], down_v, wsem.at[2]),
+    ]
     f32 = jnp.float32
     bf16 = jnp.bfloat16
-    block = 64
+    for copy in inputs[:2]:
+        copy.wait()
+    out_copy.start()
     for start in range(length - block, -1, -block):
         rows = slice(start, start + block)
         gated = value_ref[rows].astype(f32) / (1.0 + jnp.exp(-gate_ref[rows].astype(f32)))
@@ -195,18 +221,17 @@
         glued[lead + start : lead + start + block] = gated.astype(f32)
         if start == length - block:
             hsend[...] = gated[block - lead :]
-    pl.semaphore_wait(barrier, len(ORDER) + peers + 1)
-    halo().start()
-
-    lane = lax.broadcasted_iota(jnp.int32, (tokens, 128), 1)
+    for copy in inputs[2:5]:
+        copy.wait()
     picks = pick_ref[...].astype(f32)
     logits = logit_ref[...]
-    cols = [picks[:, 0:1], picks[:, 1:2], logits[:, 0:1], logits[:, 1:2]]
-    wide = jnp.zeros((tokens, 128), f32)
-    for k in range(4):
-        wide = jnp.where(lane == k, cols[k], wide)
-    tall = wide.T
-    rows_of = [tall[k : k + 1, :] for k in range(4)]
+    rows_of = [picks[0:1, :], picks[1:2, :], logits[0:1, :], logits[1:2, :]]
+    sublane = lax.broadcasted_iota(jnp.int32, (128, tokens), 0)
+    tall = jnp.zeros((128, tokens), f32)
+    for k in range(2):
+        tall = jnp.where(sublane == k, rows_of[k], tall)
+    wide = tall.T
+    cols = [wide[:, 0:1], wide[:, 1:2]]
     square = (tokens, tokens)
     earlier = lax.broadcasted_iota(jnp.int32, square, 0) < lax.broadcasted_iota(
         jnp.int32, square, 1
@@ -256,30 +281,61 @@
         meta_ref[d, 1:2, :group_rows] = part[3:4] * slot + part[4:5] + empty
         meta_ref[d, 2:3, :group_rows] = part[5:6] + part[6:7] + part[7:8]
         meta_ref[d, 3:4, :group_rows] = part[8:9] + part[9:10] + part[10:11]
-    for d in ORDER:
-        mcopy(d).start()
-
+    for copy in inputs[5:]:
+        copy.wait()
+    for copy in weights:
+        copy.start()
     wide_group = channels * n_tp // CONV_GROUPS
     taps = taps_ref[...].astype(f32)
-    for start in range(length - block, -1, -block):
+    spans = [(start, block) for start in range(length - block, 0, -block)]
+    spans += [(block // 2, block // 2), (0, block // 2)]
+    for start, size in spans:
+        if start == length - block * 2:
+            pl.semaphore_wait(
+                barrier,
+                len(ORDER) + peers - 1
+                + jnp.where(head_dev, 0, 1) + jnp.where(tail_dev, 0, 1),
+            )
+
+            @pl.when(jnp.logical_not(tail_dev))
+            def _():
+                halo().start()
+
+            for d in ORDER:
+                mcopy(d).start()
         if start == 0:
-            halo().wait_recv()
-            keep = jnp.where(sp > 0, 1.0, 0.0)
-            glued[:lead] = hrecv[...].astype(f32) * keep
+
+            @pl.when(head_dev)
+            def _():
+                glued[:lead] = jnp.zeros((lead, channels), f32)
+
+            @pl.when(jnp.logical_not(head_dev))
+            def _():
+                halo().wait_recv()
+                glued[:lead] = hrecv[...].astype(f32)
+
         for low_lane in range(0, channels, wide_group):
             part = slice(low_lane, low_lane + wide_group)
-            total = jnp.zeros((block, wide_group), f32) + bias_ref[:, part]
+            total = jnp.zeros((size, wide_group), f32) + bias_ref[:, part]
             for offset in range(reach + 1):
                 first = start + lead - reach + offset
-                total += taps[offset : offset + 1, part] * glued[first : first + block, part]
+                total += taps[offset : offset + 1, part] * glued[first : first + size, part]
             centre = jnp.mean(total, axis=-1, keepdims=True)
             total = total - centre
             variance = jnp.mean(total * total, axis=-1, keepdims=True)
             level = total * lax.rsqrt(variance + EPS)
             level = level * gain_ref[:, part] + shift_ref[:, part]
-            mixed[start : start + block, part] = (level / (1.0 + jnp.exp(-level))).astype(bf16)
-    for o in range(1, n_tp):
-        tcopy(o).start()
+            mixed[start : start + size, part] = (level / (1.0 + jnp.exp(-level))).astype(bf16)
+        if start + size == length:
+            continue
+        pieces = (start,) if start + size + block < length else (start, start + size)
+        for piece in pieces:
+            for o in range(1, n_tp):
+
+                @pl.when((tp + o) % n_tp == piece // tokens)
+                def _():
+                    tcopy(o, piece % tokens, size).start()
+
     out_copy.wait()
 
     def weight_rows(which):
@@ -287,8 +343,26 @@
 
     own = mixed[pl.ds(pl.multiple_of(tp * tokens, tokens), tokens), :]
     proj[...] = jnp.dot(own, weight_rows(tp), preferred_element_type=f32)
+
+    def arrivals(act):
+        for who in range(n_tp):
+            for start, size in spans:
+                if start // tokens == who:
+                    for o in range(1, n_tp):
+                        act(who, o, start % tokens, size)
+
+    def landed(who, o, begin, size):
+        @pl.when(tp == who)
+        def _():
+            tcopy(o, begin, size).wait_recv()
+
+    def left(who, o, begin, size):
+        @pl.when((tp + o) % n_tp == who)
+        def _():
+            tcopy(o, begin, size).wait_send()
+
+    arrivals(landed)
     for o in range(1, n_tp):
-        tcopy(o).wait_recv()
         proj[...] += jnp.dot(
             mrest[o], weight_rows((tp + n_tp - o) % n_tp), preferred_element_type=f32
         )
@@ -300,6 +374,7 @@
         scale = lax.rsqrt(jnp.mean(full * full, axis=-1, keepdims=True) + EPS)
         normed_ref[rows] = (full * scale * ffn_ref[...]).astype(bf16)
 
+    inner = (z >= 1) & (z < PLANES - 1)
     for d in ORDER + (0,):
         for h in range(HALVES):
             picked = jnp.dot(
@@ -308,8 +383,14 @@
                 preferred_element_type=f32,
             )
             zsend[d, h] = picked.astype(bf16)
-            if d:
+            if d == 1:
                 zcopy(d, h).start()
+            elif d:
+
+                @pl.when(inner)
+                def _():
+                    zcopy(d, h).start()
+
 
     def places(d):
         meta = meta_ref[0] if d == 0 else mrecv[d]
@@ -355,16 +436,19 @@
             answer = answer.astype(jnp.bfloat16)
             arecv[d, h, :slot] = answer[:slot]
             asend[d, h, slot:] = answer[slot:]
+
+    def reply(d, halves=tuple(range(HALVES))):
+        for h in halves:
             for o in range(1, peers):
                 acopy(d, h, o).start()
 
-    def combine(d):
+    def combine(d, halves=tuple(range(HALVES))):
         at, shares = places(d)
         mix = jnp.where(at[0], shares[0], 0.0) + jnp.where(at[1], shares[1], 0.0)
         high = mix.astype(jnp.bfloat16)
         low = (mix - high.astype(jnp.float32)).astype(jnp.bfloat16)
         dims = (((0,), (0,)), ((), ()))
-        for h in range(HALVES):
+        for h in halves:
             for o in range(1, peers):
                 acopy(d, h, o).wait_recv()
             answers = arecv[d, h]
@@ -376,41 +460,61 @@
                 csend[d, h] = total.astype(jnp.bfloat16)
                 ccopy(d, h).start()
 
-    a, b, c = ORDER
+    head, rest = (0,), tuple(range(1, HALVES))
     entry(0)
-    entry(a)
-    for copy in weights:
-        copy.wait()
-    expert(0)
-    entry(b)
-    inner = (z >= 1) & (z < PLANES - 1)
 
     @pl.when(inner)
     def _():
-        expert(a)
+        entry(3)
+        entry(1)
+        for copy in weights:
+            copy.wait()
+        expert(0)
+        expert(3)
+        reply(3)
+        expert(1)
+        entry(2)
+        reply(1, head)
+        combine(3)
+        expert(2)
+        reply(2)
+        reply(1, rest)
+        combine(1, head)
+        combine(2, head)
+        reply(0)
+        combine(2, rest)
+        combine(1, rest)
         combine(0)
-        expert(b)
-        combine(a)
-        combine(b)
-        entry(c)
-        expert(c)
-        combine(c)
 
     @pl.when(jnp.logical_not(inner))
     def _():
-        expert(a)
+        entry(1)
+        for copy in weights:
+            copy.wait()
+        expert(0)
+        for d in (2, 3):
+            for h in range(HALVES):
+                zcopy(d, h).start()
+        entry(2)
+        expert(1)
+        reply(1, head)
+        expert(2)
+        reply(2)
+        entry(3)
+        reply(1, rest)
+        combine(2)
+        combine(1, head)
+        expert(3)
+        reply(3)
+        combine(1, rest)
+        reply(0)
+        combine(3)
         combine(0)
-        entry(c)
-        combine(a)
-        expert(b)
-        expert(c)
-        combine(b)
-        combine(c)
 
     dims = (((0,), (0,)), ((), ()))
     for h in range(HALVES):
         total = hidden_ref[:, span(h)].astype(jnp.float32)
-        for d in (0,) + ORDER:
+        for d in (2, 1, 3, 0):
             if d:
                 ccopy(d, h).wait_recv()
             total += lax.dot_general(
@@ -421,9 +525,11 @@
             )
         out_ref[:, span(h)] = total.astype(jnp.bfloat16)
 
-    halo().wait_send()
-    for o in range(1, n_tp):
-        tcopy(o).wait_send()
+    @pl.when(jnp.logical_not(tail_dev))
+    def _():
+        halo().wait_send()
+
+    arrivals(left)
     for d in ORDER:
         mcopy(d).wait_send()
         for h in range(HALVES):
@@ -470,10 +576,22 @@
     dma = pltpu.SemaphoreType.DMA
     return pl.pallas_call(
         functools.partial(layer_kernel, cap, slot),
-        out_shape=jax.ShapeDtypeStruct((rows, width), bf16),
-        in_specs=[vmem] * 11 + [hbm] * 4,
+        out_shape=pltpu.VMEM((rows, width), bf16),
+        in_specs=[hbm] * 15,
         out_specs=vmem,
         scratch_shapes=[
+            pltpu.VMEM(glu_value.shape, bf16),
+            pltpu.VMEM(glu_gate.shape, bf16),
+            pltpu.VMEM(conv_kernel.shape, bf16),
+            pltpu.VMEM((1, channels), f32),
+            pltpu.VMEM((1, channels), f32),
+            pltpu.VMEM((1, channels), f32),
+            pltpu.VMEM((rows, width), bf16),
+            pltpu.VMEM((1, width), f32),
+            pltpu.VMEM((2, rows), jnp.int32),
+            pltpu.VMEM((2, rows), f32),
+            pltpu.VMEM((1, rows), f32),
+            dma((11,)),
             pltpu.VMEM((lead + length, channels), f32),
             pltpu.VMEM((lead, channels), bf16),
             pltpu.VMEM((lead, channels), bf16),
@@ -500,8 +618,8 @@
             dma((4,)),
             dma((1,)),
             dma((1,)),
-            dma((n_tp,)),
-            dma((n_tp,)),
+            dma((n_tp, rows // 32)),
+            dma((n_tp, rows // 32)),
             dma((PLANES, HALVES)),
             dma((PLANES, HALVES)),
             dma((PLANES,)),
@@ -525,8 +643,8 @@
         group_shift[None, :],
         residual,
         ffn_gain[None, :],
-        expert_pick,
-        pair_logits,
+        expert_pick.T,
+        pair_logits.T,
         group_prob[None, :],
         out_weight,
         gate_weight,

time: 80.9 us -> 73 us (0.902)
  Pallas kernels: 76 us -> 72 us
  local copies, waits for them, and re-layouts: 4.7 us -> 0.8 us
    pallas_call x1, Pallas kernels: 76 us -> 72 us  [local(): pl.pallas_call(functools.partial(layer_kernel, cap, slot), out_shape=pltp...]
    unnamed x3 -> x1, local copies, waits for them, and re-layouts: 4.7 us -> 0.8 us
where the time goes in v1:
time: 73 us; the launch traced here: 72.8 us
  Pallas kernels  72 us (99%)
  local copies, waits for them, and re-layouts  0.8 us (1%)
    pallas_call x1, Pallas kernels, local(): pl.pallas_call(functools.partial(layer_kernel, cap, slot), out_shape=pltp...  72 us

profile of v1, /device:TPU:0, one launch (start us, length us, event | category | flops | bytes accessed | tf_op | source)
XLA Modules:
  0.0 72.8 jit_solution(1799841135596975131)
XLA Ops:
  0.0 72.0 %shard_map.145 = bf16[128,2048]{1,0:T(8,128)(2,1)S(1)} custom-call(bf16[256,512]{1,0:T(8,128)(2,1)} %value_hbm.1, bf16[256,512]{1,0:T(8,128)(2,1)} %glu_gate_hbm.1, bf16[31,512]{1,0:T(8,128)(2,1)} %taps_hbm.1, f32[1,512]{1,0:T(1,128)} %bitcast.8, f32[1,512]{1,0:T(1,128)} %bitcast.9, f32[1,512]{1,0:T(1,128)} %bitcast.10, bf16[128,2048]{1,0:T(8,128)(2,1)} %residual_hbm.1, ...), custom_call_target="tpu_custom_call" | custom-call | tf_op jit(solution)/shard_map/pallas_call | solution.py:577
  72.0 0.8 %copy.17 = bf16[128,2048]{1,0:T(8,128)(2,1)} copy(bf16[128,2048]{1,0:T(8,128)(2,1)S(1)} %shard_map.145) | data formatting | bytes 1048576

commit v2 on v1

--- a/solution.py
+++ b/solution.py
@@ -287,22 +287,33 @@
         copy.start()
     wide_group = channels * n_tp // CONV_GROUPS
     taps = taps_ref[...].astype(f32)
+    def enter():
+        pl.semaphore_wait(
+            barrier,
+            len(ORDER) + peers - 1
+            + jnp.where(head_dev, 0, 1) + jnp.where(tail_dev, 0, 1),
+        )
+
+        @pl.when(jnp.logical_not(tail_dev))
+        def _():
+            halo().start()
+
+        for d in ORDER:
+            mcopy(d).start()
+
+    @pl.when(z > 0)
+    def _():
+        enter()
+
     spans = [(start, block) for start in range(length - block, 0, -block)]
     spans += [(block // 2, block // 2), (0, block // 2)]
     for start, size in spans:
         if start == length - block * 2:
-            pl.semaphore_wait(
-                barrier,
-                len(ORDER) + peers - 1
-                + jnp.where(head_dev, 0, 1) + jnp.where(tail_dev, 0, 1),
-            )
-
-            @pl.when(jnp.logical_not(tail_dev))
+
+            @pl.when(z == 0)
             def _():
-                halo().start()
-
-            for d in ORDER:
-                mcopy(d).start()
+                enter()
+
         if start == 0:
 
             @pl.when(head_dev)
@@ -404,7 +415,7 @@
         shares = [meta[2 + k : 3 + k, :group_rows] for k in range(2)]
         return out, shares
 
-    def entry(d):
+    def entry(d, after=()):
         if d:
             mcopy(d).wait_recv()
         at, _ = places(d)
@@ -412,6 +423,15 @@
         for h in range(HALVES):
             if d:
                 zcopy(d, h).wait_recv()
+            for who in range(n_tp if after else 0):
+                if h == min(who, HALVES - 1):
+
+                    @pl.when(tp == who)
+                    def _():
+                        for later in after:
+                            for k in range(HALVES):
+                                zcopy(later, k).start()
+
             rows = zsend[0, h] if d == 0 else zrecv[d, h]
             spread = jnp.dot(chosen, rows, preferred_element_type=jnp.float32)
             spread = spread.astype(jnp.bfloat16)
@@ -473,17 +493,16 @@
         expert(3)
         reply(3)
         expert(1)
-        entry(2)
         reply(1, head)
         combine(3)
+        entry(2)
+        reply(1, rest)
+        combine(1, head)
         expert(2)
         reply(2)
-        reply(1, rest)
-        combine(1, head)
-        combine(2, head)
+        combine(1, rest)
         reply(0)
-        combine(2, rest)
-        combine(1, rest)
+        combine(2)
         combine(0)
 
     @pl.when(jnp.logical_not(inner))
@@ -492,23 +511,18 @@
         for copy in weights:
             copy.wait()
         expert(0)
-        for d in (2, 3):
-            for h in range(HALVES):
-                zcopy(d, h).start()
-        entry(2)
+        entry(2, after=(3, 2))
         expert(1)
-        reply(1, head)
+        entry(3)
         expert(2)
         reply(2)
-        entry(3)
-        reply(1, rest)
-        combine(2)
-        combine(1, head)
         expert(3)
         reply(3)
-        combine(1, rest)
+        combine(2)
+        reply(1)
+        combine(3)
         reply(0)
-        combine(3)
+        combine(1)
         combine(0)
 
     dims = (((0,), (0,)), ((), ()))

time: 73 us -> 66.6 us (0.912)
  Pallas kernels: 72 us -> 65.7 us
    pallas_call x1, Pallas kernels: 72 us -> 65.7 us  [local(): pl.pallas_call(functools.partial(layer_kernel, cap, slot), out_shape=pltp...]
where the time goes in v2:
time: 66.6 us; the launch traced here: 66.5 us
  Pallas kernels  65.7 us (99%)
  local copies, waits for them, and re-layouts  0.8 us (1%)
    pallas_call x1, Pallas kernels, local(): pl.pallas_call(functools.partial(layer_kernel, cap, slot), out_shape=pltp...  65.7 us

profile of v2, /device:TPU:0, one launch (start us, length us, event | category | flops | bytes accessed | tf_op | source)
XLA Modules:
  0.0 66.5 jit_solution(4415397811761084016)
XLA Ops:
  0.0 65.7 %shard_map.145 = bf16[128,2048]{1,0:T(8,128)(2,1)S(1)} custom-call(bf16[256,512]{1,0:T(8,128)(2,1)} %value_hbm.1, bf16[256,512]{1,0:T(8,128)(2,1)} %glu_gate_hbm.1, bf16[31,512]{1,0:T(8,128)(2,1)} %taps_hbm.1, f32[1,512]{1,0:T(1,128)} %bitcast.8, f32[1,512]{1,0:T(1,128)} %bitcast.9, f32[1,512]{1,0:T(1,128)} %bitcast.10, bf16[128,2048]{1,0:T(8,128)(2,1)} %residual_hbm.1, ...), custom_call_target="tpu_custom_call" | custom-call | tf_op jit(solution)/shard_map/pallas_call | solution.py:591
  65.7 0.8 %copy.17 = bf16[128,2048]{1,0:T(8,128)(2,1)} copy(bf16[128,2048]{1,0:T(8,128)(2,1)S(1)} %shard_map.145) | data formatting | bytes 1048576

commit v3 on v2

--- a/solution.py
+++ b/solution.py
@@ -59,7 +59,6 @@
     place_ref,
     meta_ref,
     normed_ref,
-    hidden_ref,
     proj,
     out_v,
     zsend,
@@ -165,6 +164,7 @@
             device_id=((sp + 1) % n_sp, tp), device_id_type=MESH,
         )
 
+    wide_group = channels * n_tp // CONV_GROUPS
     block = 64
 
     def tcopy(o, begin, size):
@@ -179,8 +179,14 @@
 
     head_dev, tail_dev = sp == 0, sp == n_sp - 1
     barrier = pltpu.get_barrier_semaphore()
-    for d in ORDER:
-        pl.semaphore_signal(barrier, inc=1, device_id=mate(d), device_id_type=MESH)
+    inner = (z >= 1) & (z < PLANES - 1)
+    outer = jnp.logical_not(inner)
+    pl.semaphore_signal(barrier, inc=1, device_id=mate(1), device_id_type=MESH)
+
+    @pl.when(inner)
+    def _():
+        pl.semaphore_signal(barrier, inc=1, device_id=mate(3), device_id_type=MESH)
+
     for o in range(1, peers):
         pl.semaphore_signal(
             barrier, inc=1, device_id=peer((j + o) % peers), device_id_type=MESH
@@ -218,7 +224,9 @@
         rows = slice(start, start + block)
         gated = value_ref[rows].astype(f32) / (1.0 + jnp.exp(-gate_ref[rows].astype(f32)))
         gated = gated.astype(bf16)
-        glued[lead + start : lead + start + block] = gated.astype(f32)
+        for k in range(channels // wide_group):
+            piece = gated[:, k * wide_group : (k + 1) * wide_group]
+            glued[k, lead + start : lead + start + block] = piece.astype(f32)
         if start == length - block:
             hsend[...] = gated[block - lead :]
     for copy in inputs[2:5]:
@@ -285,12 +293,11 @@
         copy.wait()
     for copy in weights:
         copy.start()
-    wide_group = channels * n_tp // CONV_GROUPS
     taps = taps_ref[...].astype(f32)
     def enter():
         pl.semaphore_wait(
             barrier,
-            len(ORDER) + peers - 1
+            peers + jnp.where(inner, 1, 0)
             + jnp.where(head_dev, 0, 1) + jnp.where(tail_dev, 0, 1),
         )
 
@@ -298,39 +305,37 @@
         def _():
             halo().start()
 
-        for d in ORDER:
-            mcopy(d).start()
-
-    @pl.when(z > 0)
-    def _():
-        enter()
+        mcopy(1).start()
+
+        @pl.when(inner)
+        def _():
+            mcopy(3).start()
 
     spans = [(start, block) for start in range(length - block, 0, -block)]
     spans += [(block // 2, block // 2), (0, block // 2)]
     for start, size in spans:
         if start == length - block * 2:
-
-            @pl.when(z == 0)
-            def _():
-                enter()
+            enter()
 
         if start == 0:
 
             @pl.when(head_dev)
             def _():
-                glued[:lead] = jnp.zeros((lead, channels), f32)
+                glued[:, :lead] = jnp.zeros((channels // wide_group, lead, wide_group), f32)
 
             @pl.when(jnp.logical_not(head_dev))
             def _():
                 halo().wait_recv()
-                glued[:lead] = hrecv[...].astype(f32)
+                for k in range(channels // wide_group):
+                    piece = hrecv[:, k * wide_group : (k + 1) * wide_group]
+                    glued[k, :lead] = piece.astype(f32)
 
         for low_lane in range(0, channels, wide_group):
             part = slice(low_lane, low_lane + wide_group)
             total = jnp.zeros((size, wide_group), f32) + bias_ref[:, part]
             for offset in range(reach + 1):
                 first = start + lead - reach + offset
-                total += taps[offset : offset + 1, part] * glued[first : first + size, part]
+                total += taps[offset : offset + 1, part] * glued[low_lane // wide_group, first : first + size]
             centre = jnp.mean(total, axis=-1, keepdims=True)
             total = total - centre
             variance = jnp.mean(total * total, axis=-1, keepdims=True)
@@ -380,28 +385,10 @@
     for start in range(0, tokens, 16):
         rows = slice(start, start + 16)
         hidden = (residual_ref[rows].astype(f32) + proj[rows]).astype(bf16)
-        hidden_ref[rows] = hidden
         full = hidden.astype(f32)
+        proj[rows] = full
         scale = lax.rsqrt(jnp.mean(full * full, axis=-1, keepdims=True) + EPS)
         normed_ref[rows] = (full * scale * ffn_ref[...]).astype(bf16)
-
-    inner = (z >= 1) & (z < PLANES - 1)
-    for d in ORDER + (0,):
-        for h in range(HALVES):
-            picked = jnp.dot(
-                place_ref[d * group_rows : (d + 1) * group_rows, :],
-                normed_ref[:, span(h)],
-                preferred_element_type=f32,
-            )
-            zsend[d, h] = picked.astype(bf16)
-            if d == 1:
-                zcopy(d, h).start()
-            elif d:
-
-                @pl.when(inner)
-                def _():
-                    zcopy(d, h).start()
-
 
     def places(d):
         meta = meta_ref[0] if d == 0 else mrecv[d]
@@ -415,30 +402,63 @@
         shares = [meta[2 + k : 3 + k, :group_rows] for k in range(2)]
         return out, shares
 
-    def entry(d, after=()):
-        if d:
+    def chosen(d):
+        at, _ = places(d)
+        return jnp.where(at[0] | at[1], 1.0, 0.0).astype(jnp.bfloat16)
+
+    def spread(d, h, pick):
+        rows = zsend[0, h] if d == 0 else zrecv[d, h]
+        wide = jnp.dot(pick, rows, preferred_element_type=jnp.float32)
+        wide = wide.astype(jnp.bfloat16)
+        xrecv[d, h, :slot] = wide[:slot]
+        xsend[d, h, slot:] = wide[slot:]
+        for o in range(1, peers):
+            xcopy(d, h, o).start()
+
+    def gather(d, h):
+        picked = jnp.dot(
+            place_ref[d * group_rows : (d + 1) * group_rows, :],
+            normed_ref[:, span(h)],
+            preferred_element_type=f32,
+        )
+        zsend[d, h] = picked.astype(bf16)
+
+    def dispatch(d, h):
+        gather(d, h)
+        if d == 1:
+            zcopy(d, h).start()
+        elif d == 3:
+
+            @pl.when(inner)
+            def _():
+                zcopy(d, h).start()
+
+    own_pick = chosen(0)
+    for h in range(HALVES):
+        gather(0, h)
+        spread(0, h, own_pick)
+        dispatch(3, h)
+        dispatch(1, h)
+    for h in range(HALVES):
+        dispatch(2, h)
+
+    def entry(d, after=(), halves=tuple(range(HALVES))):
+        if halves[0] == 0:
             mcopy(d).wait_recv()
-        at, _ = places(d)
-        chosen = jnp.where(at[0] | at[1], 1.0, 0.0).astype(jnp.bfloat16)
-        for h in range(HALVES):
-            if d:
-                zcopy(d, h).wait_recv()
+        pick = chosen(d)
+        for h in halves:
+            zcopy(d, h).wait_recv()
             for who in range(n_tp if after else 0):
                 if h == min(who, HALVES - 1):
 
                     @pl.when(tp == who)
                     def _():
                         for later in after:
+                            mcopy(later).start()
                             for k in range(HALVES):
                                 zcopy(later, k).start()
 
-            rows = zsend[0, h] if d == 0 else zrecv[d, h]
-            spread = jnp.dot(chosen, rows, preferred_element_type=jnp.float32)
-            spread = spread.astype(jnp.bfloat16)
-            xrecv[d, h, :slot] = spread[:slot]
-            xsend[d, h, slot:] = spread[slot:]
-            for o in range(1, peers):
-                xcopy(d, h, o).start()
+            spread(d, h, pick)
 
     def expert(d):
         gate_out = None
@@ -461,6 +481,21 @@
         for h in halves:
             for o in range(1, peers):
                 acopy(d, h, o).start()
+
+    def settle(d, h, last=False):
+        if d:
+            ccopy(d, h).wait_recv()
+        total = lax.dot_general(
+            place_ref[d * group_rows : (d + 1) * group_rows, :],
+            cret[d, h],
+            (((0,), (0,)), ((), ())),
+            preferred_element_type=f32,
+        )
+        total += proj[:, span(h)]
+        if last:
+            out_ref[:, span(h)] = total.astype(bf16)
+        else:
+            proj[:, span(h)] = total
 
     def combine(d, halves=tuple(range(HALVES))):
         at, shares = places(d)
@@ -480,12 +515,27 @@
                 csend[d, h] = total.astype(jnp.bfloat16)
                 ccopy(d, h).start()
 
+    def drain():
+        @pl.when(jnp.logical_not(tail_dev))
+        def _():
+            halo().wait_send()
+
+        arrivals(left)
+        for d in ORDER:
+            mcopy(d).wait_send()
+            for h in range(HALVES):
+                zcopy(d, h).wait_send()
+        for d in range(PLANES):
+            for h in range(HALVES):
+                for o in range(1, peers):
+                    xcopy(d, h, o).wait_send()
+                    acopy(d, h, o).wait_send()
+
     head, rest = (0,), tuple(range(1, HALVES))
-    entry(0)
 
     @pl.when(inner)
     def _():
-        entry(3)
+        entry(3, after=(2,))
         entry(1)
         for copy in weights:
             copy.wait()
@@ -501,11 +551,21 @@
         expert(2)
         reply(2)
         combine(1, rest)
+        combine(2, head)
         reply(0)
-        combine(2)
-        combine(0)
-
-    @pl.when(jnp.logical_not(inner))
+        combine(2, rest)
+        for h in range(HALVES):
+            settle(3, h)
+        for h in range(HALVES):
+            combine(0, (h,))
+            settle(0, h)
+        drain()
+        for h in range(HALVES):
+            settle(1, h)
+        for h in range(HALVES):
+            settle(2, h, last=True)
+
+    @pl.when(outer)
     def _():
         entry(1)
         for copy in weights:
@@ -514,46 +574,35 @@
         entry(2, after=(3, 2))
         expert(1)
         entry(3)
+        reply(1, head)
         expert(2)
-        reply(2)
+        reply(2, head)
         expert(3)
         reply(3)
-        combine(2)
-        reply(1)
+        combine(1, head)
+        combine(2, head)
+        reply(1, rest)
+        reply(0, head)
         combine(3)
-        reply(0)
-        combine(1)
-        combine(0)
-
-    dims = (((0,), (0,)), ((), ()))
-    for h in range(HALVES):
-        total = hidden_ref[:, span(h)].astype(jnp.float32)
-        for d in (2, 1, 3, 0):
-            if d:
-                ccopy(d, h).wait_recv()
-            total += lax.dot_general(
-                place_ref[d * group_rows : (d + 1) * group_rows, :],
-                cret[d, h],
-                dims,
-                preferred_element_type=jnp.float32,
-            )
-        out_ref[:, span(h)] = total.astype(jnp.bfloat16)
-
-    @pl.when(jnp.logical_not(tail_dev))
-    def _():
-        halo().wait_send()
-
-    arrivals(left)
+        reply(2, rest)
+        combine(1, rest)
+        reply(0, rest)
+        combine(0, head)
+        combine(2, rest)
+        settle(0, 0)
+        combine(0, rest)
+        for h in rest:
+            settle(0, h)
+        drain()
+        for h in range(HALVES):
+            settle(3, h)
+            settle(1, h)
+        for h in range(HALVES):
+            settle(2, h, last=True)
+
     for d in ORDER:
-        mcopy(d).wait_send()
-        for h in range(HALVES):
-            zcopy(d, h).wait_send()
+        for h in range(HALVES):
             ccopy(d, h).wait_send()
-    for d in range(PLANES):
-        for h in range(HALVES):
-            for o in range(1, peers):
-                xcopy(d, h, o).wait_send()
-                acopy(d, h, o).wait_send()
 
 
 def local(
@@ -582,6 +631,7 @@
     group_rows = peers * cap // 2
     slot = max(cap, ROWS_MIN)
     slots = peers * slot
+    wide_group = channels * n_tp // CONV_GROUPS
     lead = -(-(conv_kernel.shape[0] - 1) // 16) * 16
     bf16 = jnp.bfloat16
     f32 = jnp.float32
@@ -606,14 +656,13 @@
             pltpu.VMEM((2, rows), f32),
             pltpu.VMEM((1, rows), f32),
             dma((11,)),
-            pltpu.VMEM((lead + length, channels), f32),
+            pltpu.VMEM((channels // wide_group, lead + length, wide_group), f32),
             pltpu.VMEM((lead, channels), bf16),
             pltpu.VMEM((lead, channels), bf16),
             pltpu.VMEM((length, channels), bf16),
             pltpu.VMEM((n_tp, rows, channels), bf16),
             pltpu.VMEM((PLANES * group_rows, rows), bf16),
             pltpu.VMEM((PLANES, 8, 128), f32),
-            pltpu.VMEM((rows, width), bf16),
             pltpu.VMEM((rows, width), bf16),
             pltpu.VMEM((rows, width), f32),
             pltpu.VMEM(out_weight.shape, bf16),

time: 66.6 us -> 64.9 us (0.974)
  Pallas kernels: 65.7 us -> 63.9 us
    pallas_call x1, Pallas kernels: 65.7 us -> 63.9 us  [local(): pl.pallas_call(functools.partial(layer_kernel, cap, slot), out_shape=pltp...]
where the time goes in v3:
time: 64.9 us; the launch traced here: 64.7 us
  Pallas kernels  63.9 us (98%)
  local copies, waits for them, and re-layouts  0.8 us (1%)
    pallas_call x1, Pallas kernels, local(): pl.pallas_call(functools.partial(layer_kernel, cap, slot), out_shape=pltp...  63.9 us

profile of v3, /device:TPU:0, one launch (start us, length us, event | category | flops | bytes accessed | tf_op | source)
XLA Modules:
  0.0 64.7 jit_solution(1119986040111023569)
XLA Ops:
  0.0 63.9 %shard_map.145 = bf16[128,2048]{1,0:T(8,128)(2,1)S(1)} custom-call(bf16[256,512]{1,0:T(8,128)(2,1)} %value_hbm.1, bf16[256,512]{1,0:T(8,128)(2,1)} %glu_gate_hbm.1, bf16[31,512]{1,0:T(8,128)(2,1)} %taps_hbm.1, f32[1,512]{1,0:T(1,128)} %bitcast.8, f32[1,512]{1,0:T(1,128)} %bitcast.9, f32[1,512]{1,0:T(1,128)} %bitcast.10, bf16[128,2048]{1,0:T(8,128)(2,1)} %residual_hbm.1, ...), custom_call_target="tpu_custom_call" | custom-call | tf_op jit(solution)/shard_map/pallas_call | solution.py:641
  63.9 0.8 %copy.17 = bf16[128,2048]{1,0:T(8,128)(2,1)} copy(bf16[128,2048]{1,0:T(8,128)(2,1)S(1)} %shard_map.145) | data formatting | bytes 1048576

commit v4 on v3

--- a/solution.py
+++ b/solution.py
@@ -73,7 +73,6 @@
     gate_v,
     up_v,
     down_v,
-    wsem,
     hss,
     hrs,
     tss,
@@ -125,20 +124,20 @@
     def zcopy(d, h):
         return pltpu.make_async_remote_copy(
             src_ref=zsend.at[d, h], dst_ref=zrecv.at[d, h],
-            send_sem=zss.at[d, h], recv_sem=zrs.at[d, h],
+            send_sem=zss.at[0], recv_sem=zrs.at[d - 1, h],
             device_id=mate(d), device_id_type=MESH,
         )
 
     def mcopy(d):
         return pltpu.make_async_remote_copy(
-            src_ref=meta_ref.at[d], dst_ref=mrecv.at[d], send_sem=mss.at[d], recv_sem=mrs.at[d],
+            src_ref=meta_ref.at[d], dst_ref=mrecv.at[d], send_sem=mss.at[0], recv_sem=mrs.at[d - 1],
             device_id=mate(d), device_id_type=MESH,
         )
 
     def ccopy(d, h):
         return pltpu.make_async_remote_copy(
             src_ref=csend.at[d, h], dst_ref=cret.at[d, h],
-            send_sem=css.at[d, h], recv_sem=crs.at[d, h],
+            send_sem=css.at[0], recv_sem=crs.at[d - 1, h],
             device_id=mate(d), device_id_type=MESH,
         )
 
@@ -146,16 +145,38 @@
         rows = pl.ds(o * slot, slot)
         return pltpu.make_async_remote_copy(
             src_ref=xsend.at[d, h, rows], dst_ref=xrecv.at[d, h, rows],
-            send_sem=xss.at[d, h, o], recv_sem=xrs.at[d, h, o],
+            send_sem=xss.at[0], recv_sem=xrs.at[d, h],
             device_id=peer((j + o) % peers), device_id_type=MESH,
+        )
+
+    def xall(d, h):
+        rows = pl.ds(slot, slots - slot)
+        return pltpu.make_async_remote_copy(
+            src_ref=xsend.at[d, h, rows], dst_ref=xrecv.at[d, h, rows],
+            send_sem=xss.at[0], recv_sem=xrs.at[d, h],
+            device_id=peer((j + 1) % peers), device_id_type=MESH,
         )
 
     def acopy(d, h, o):
         rows = pl.ds(o * slot, slot)
         return pltpu.make_async_remote_copy(
             src_ref=asend.at[d, h, rows], dst_ref=arecv.at[d, h, rows],
-            send_sem=ass.at[d, h, o], recv_sem=ars.at[d, h, o],
+            send_sem=ass.at[0], recv_sem=ars.at[d, h],
             device_id=peer((j + peers - o) % peers), device_id_type=MESH,
+        )
+
+    def aall(d, h):
+        rows = pl.ds(slot, slots - slot)
+        return pltpu.make_async_remote_copy(
+            src_ref=asend.at[d, h, rows], dst_ref=arecv.at[d, h, rows],
+            send_sem=ass.at[0], recv_sem=ars.at[d, h],
+            device_id=peer((j + peers - 1) % peers), device_id_type=MESH,
+        )
+
+    def sent(src, sem, recv_sem):
+        return pltpu.make_async_remote_copy(
+            src_ref=src, dst_ref=src, send_sem=sem.at[0], recv_sem=recv_sem,
+            device_id=mate(1), device_id_type=MESH,
         )
 
     def halo():
@@ -170,10 +191,9 @@
     def tcopy(o, begin, size):
         other = (tp + o) % n_tp
         rows = pl.ds(pl.multiple_of(other * tokens + begin, size), size)
-        mark = begin // (block // 2)
         return pltpu.make_async_remote_copy(
             src_ref=mixed.at[rows], dst_ref=mrest.at[o, pl.ds(begin, size)],
-            send_sem=tss.at[o, mark], recv_sem=trs.at[o, mark],
+            send_sem=tss.at[o - 1], recv_sem=trs.at[o - 1],
             device_id=(sp, other), device_id_type=MESH,
         )
 
@@ -209,11 +229,11 @@
     inputs = [pltpu.make_async_copy(a, b, isem.at[k]) for k, (a, b) in enumerate(sources)]
     for copy in inputs:
         copy.start()
-    out_copy = pltpu.make_async_copy(out_hbm, out_v, wsem.at[3])
+    out_copy = pltpu.make_async_copy(out_hbm, out_v, isem.at[0])
     weights = [
-        pltpu.make_async_copy(gate_hbm.at[0], gate_v, wsem.at[0]),
-        pltpu.make_async_copy(up_hbm.at[0], up_v, wsem.at[1]),
-        pltpu.make_async_copy(down_hbm.at[0], down_v, wsem.at[2]),
+        pltpu.make_async_copy(gate_hbm.at[0], gate_v, isem.at[5]),
+        pltpu.make_async_copy(up_hbm.at[0], up_v, isem.at[6]),
+        pltpu.make_async_copy(down_hbm.at[0], down_v, isem.at[7]),
     ]
     f32 = jnp.float32
     bf16 = jnp.bfloat16
@@ -360,24 +380,8 @@
     own = mixed[pl.ds(pl.multiple_of(tp * tokens, tokens), tokens), :]
     proj[...] = jnp.dot(own, weight_rows(tp), preferred_element_type=f32)
 
-    def arrivals(act):
-        for who in range(n_tp):
-            for start, size in spans:
-                if start // tokens == who:
-                    for o in range(1, n_tp):
-                        act(who, o, start % tokens, size)
-
-    def landed(who, o, begin, size):
-        @pl.when(tp == who)
-        def _():
-            tcopy(o, begin, size).wait_recv()
-
-    def left(who, o, begin, size):
-        @pl.when((tp + o) % n_tp == who)
-        def _():
-            tcopy(o, begin, size).wait_send()
-
-    arrivals(landed)
+    for o in range(1, n_tp):
+        tcopy(o, 0, tokens).wait_recv()
     for o in range(1, n_tp):
         proj[...] += jnp.dot(
             mrest[o], weight_rows((tp + n_tp - o) % n_tp), preferred_element_type=f32
@@ -463,8 +467,7 @@
     def expert(d):
         gate_out = None
         for h in range(HALVES):
-            for o in range(1, peers):
-                xcopy(d, h, o).wait_recv()
+            xall(d, h).wait_recv()
             rows = xrecv[d, h]
             gate_part = jnp.dot(rows, gate_v[span(h), :], preferred_element_type=jnp.float32)
             up_part = jnp.dot(rows, up_v[span(h), :], preferred_element_type=jnp.float32)
@@ -504,8 +507,7 @@
         low = (mix - high.astype(jnp.float32)).astype(jnp.bfloat16)
         dims = (((0,), (0,)), ((), ()))
         for h in halves:
-            for o in range(1, peers):
-                acopy(d, h, o).wait_recv()
+            aall(d, h).wait_recv()
             answers = arecv[d, h]
             total = lax.dot_general(high, answers, dims, preferred_element_type=jnp.float32)
             total += lax.dot_general(low, answers, dims, preferred_element_type=jnp.float32)
@@ -520,16 +522,15 @@
         def _():
             halo().wait_send()
 
-        arrivals(left)
-        for d in ORDER:
-            mcopy(d).wait_send()
-            for h in range(HALVES):
-                zcopy(d, h).wait_send()
-        for d in range(PLANES):
-            for h in range(HALVES):
-                for o in range(1, peers):
-                    xcopy(d, h, o).wait_send()
-                    acopy(d, h, o).wait_send()
+        for o in range(1, n_tp):
+            tcopy(o, 0, tokens).wait_send()
+        away = pl.ds(1, PLANES - 1)
+        rows = pl.ds(slot, slots - slot)
+        every = pl.ds(0, HALVES)
+        sent(meta_ref.at[away], mss, mrs.at[0]).wait_send()
+        sent(zsend.at[away], zss, zrs.at[0, 0]).wait_send()
+        sent(xsend.at[pl.ds(0, PLANES), every, rows], xss, xrs.at[0, 0]).wait_send()
+        sent(asend.at[pl.ds(0, PLANES), every, rows], ass, ars.at[0, 0]).wait_send()
 
     head, rest = (0,), tuple(range(1, HALVES))
 
@@ -600,9 +601,7 @@
         for h in range(HALVES):
             settle(2, h, last=True)
 
-    for d in ORDER:
-        for h in range(HALVES):
-            ccopy(d, h).wait_send()
+    sent(csend.at[pl.ds(1, PLANES - 1)], css, crs.at[0, 0]).wait_send()
 
 
 def local(
@@ -678,21 +677,20 @@
             pltpu.VMEM(gate_weight.shape[1:], bf16),
             pltpu.VMEM(up_weight.shape[1:], bf16),
             pltpu.VMEM(down_weight.shape[1:], bf16),
-            dma((4,)),
             dma((1,)),
             dma((1,)),
-            dma((n_tp, rows // 32)),
-            dma((n_tp, rows // 32)),
+            dma((n_tp - 1,)),
+            dma((n_tp - 1,)),
+            dma((1,)),
+            dma((PLANES - 1, HALVES)),
+            dma((1,)),
+            dma((PLANES - 1,)),
+            dma((1,)),
             dma((PLANES, HALVES)),
+            dma((1,)),
             dma((PLANES, HALVES)),
-            dma((PLANES,)),
-            dma((PLANES,)),
-            dma((PLANES, HALVES, peers)),
-            dma((PLANES, HALVES, peers)),
-            dma((PLANES, HALVES, peers)),
-            dma((PLANES, HALVES, peers)),
-            dma((PLANES, HALVES)),
-            dma((PLANES, HALVES)),
+            dma((1,)),
+            dma((PLANES - 1, HALVES)),
         ],
         compiler_params=pltpu.CompilerParams(
             collective_id=0, has_side_effects=True, vmem_limit_bytes=62 * 1024 * 1024

time: 64.9 us -> 62.4 us (0.961)
  Pallas kernels: 63.9 us -> 61.4 us
    pallas_call x1, Pallas kernels: 63.9 us -> 61.4 us  [local(): pl.pallas_call(functools.partial(layer_kernel, cap, slot), out_shape=pltp...]
where the time goes in v4:
time: 62.4 us; the launch traced here: 62.2 us
  Pallas kernels  61.4 us (98%)
  local copies, waits for them, and re-layouts  0.8 us (1%)
    pallas_call x1, Pallas kernels, local(): pl.pallas_call(functools.partial(layer_kernel, cap, slot), out_shape=pltp...  61.4 us

profile of v4, /device:TPU:0, one launch (start us, length us, event | category | flops | bytes accessed | tf_op | source)
XLA Modules:
  0.0 62.2 jit_solution(434756089867647417)
XLA Ops:
  0.0 61.4 %shard_map.145 = bf16[128,2048]{1,0:T(8,128)(2,1)S(1)} custom-call(bf16[256,512]{1,0:T(8,128)(2,1)} %value_hbm.1, bf16[256,512]{1,0:T(8,128)(2,1)} %glu_gate_hbm.1, bf16[31,512]{1,0:T(8,128)(2,1)} %taps_hbm.1, f32[1,512]{1,0:T(1,128)} %bitcast.8, f32[1,512]{1,0:T(1,128)} %bitcast.9, f32[1,512]{1,0:T(1,128)} %bitcast.10, bf16[128,2048]{1,0:T(8,128)(2,1)} %residual_hbm.1, ...), custom_call_target="tpu_custom_call" | custom-call | tf_op jit(solution)/shard_map/pallas_call | solution.py:640
  61.4 0.8 %copy.17 = bf16[128,2048]{1,0:T(8,128)(2,1)} copy(bf16[128,2048]{1,0:T(8,128)(2,1)S(1)} %shard_map.145) | data formatting | bytes 1048576

commit v5 on v4

--- a/solution.py
+++ b/solution.py
@@ -597,9 +597,11 @@
         drain()
         for h in range(HALVES):
             settle(3, h)
-            settle(1, h)
-        for h in range(HALVES):
-            settle(2, h, last=True)
+        settle(1, 0)
+        settle(2, 0, last=True)
+        for h in rest:
+            settle(2, h)
+            settle(1, h, last=True)
 
     sent(csend.at[pl.ds(1, PLANES - 1)], css, crs.at[0, 0]).wait_send()
 

time: 62.4 us -> 62.6 us (level)
  no operation moved by 1% of the time
where the time goes in v5:
time: 62.6 us; the launch traced here: 62.5 us
  Pallas kernels  61.7 us (99%)
  local copies, waits for them, and re-layouts  0.8 us (1%)
    pallas_call x1, Pallas kernels, local(): pl.pallas_call(functools.partial(layer_kernel, cap, slot), out_shape=pltp...  61.7 us

profile of v5, /device:TPU:0, one launch (start us, length us, event | category | flops | bytes accessed | tf_op | source)
XLA Modules:
  0.0 62.5 jit_solution(3750067204613746536)
XLA Ops:
  0.0 61.7 %shard_map.145 = bf16[128,2048]{1,0:T(8,128)(2,1)S(1)} custom-call(bf16[256,512]{1,0:T(8,128)(2,1)} %value_hbm.1, bf16[256,512]{1,0:T(8,128)(2,1)} %glu_gate_hbm.1, bf16[31,512]{1,0:T(8,128)(2,1)} %taps_hbm.1, f32[1,512]{1,0:T(1,128)} %bitcast.8, f32[1,512]{1,0:T(1,128)} %bitcast.9, f32[1,512]{1,0:T(1,128)} %bitcast.10, bf16[128,2048]{1,0:T(8,128)(2,1)} %residual_hbm.1, ...), custom_call_target="tpu_custom_call" | custom-call | tf_op jit(solution)/shard_map/pallas_call | solution.py:642
  61.7 0.8 %copy.17 = bf16[128,2048]{1,0:T(8,128)(2,1)} copy(bf16[128,2048]{1,0:T(8,128)(2,1)S(1)} %shard_map.145) | data formatting | bytes 1048576
